TPU v7x, 32 devices: a whole 2x2x4 slice. The times are simulated.
32 devices in a mesh: ep: 8 (over z, y), tp: 4 (over x, core).
Axes of the slice: x: 2, y: 2, z: 4, core: 2. Of those that a mesh axis runs over, the one named last changes fastest.
Arguments:
- query: bfloat16 [8192, 1024], P('ep', 'tp'), may hold values from -6 to 6
- keys: bfloat16 [8192, 1024], P('ep', 'tp'), may hold values from -6 to 6
- values: bfloat16 [8192, 2048], P('ep', 'tp'), may hold values from -6 to 6
- gate_pre: bfloat16 [8192, 2048], P('ep', 'tp'), may hold values from -6 to 6
- log_decay: float32 [16, 8192], P('tp', 'ep'), may hold values from -1 to 0
- out_weight: bfloat16 [2048, 4096], P(None, 'tp'), may hold values from -0.125 to 0.125
- expert_input: bfloat16 [2048, 4096], P(('ep', 'tp')), may hold values from -6 to 6
- norm_gain: float32 [4096], replicated, may hold values from 0.1 to 1.9
- routes: int32 [2048, 2], P(('ep', 'tp')), may hold values from 0 to 7, all different within a row; in each aligned block of 64 rows (0 to 63, 64 to 127, ...) at most 24 rows name the same one
- route_weights: float32 [2048, 2], P(('ep', 'tp')), may hold values from 0.1 to 1
- w_gate: bfloat16 [8, 4096, 1536], P('ep', None, 'tp'), may hold values from -0.09375 to 0.09375
- w_up: bfloat16 [8, 4096, 1536], P('ep', None, 'tp'), may hold values from -0.09375 to 0.09375
- w_down: bfloat16 [8, 1536, 4096], P('ep', 'tp'), may hold values from -0.15625 to 0.15625
Outputs:
- mixed: bfloat16 [8192, 4096], P('ep', 'tp')
- moe_out: bfloat16 [2048, 4096], P(('ep', 'tp'))
Inputs may be any that keep to these rules, and one draw needn't show every extreme that they name: `routes`: each row names 2 different experts; among the rows of one device no expert is named by more than 24 rows, a bound that some block reaches of some device.
All inputs are finite; a program needn't handle non-finite values.
Results may differ from a plain program's by a relative error of at most 0.018.
Values may be sent and summed in bfloat16 or wider, within the bound.
A program may use at most 128 MiB of HBM per device.

v0:
```python
import functools
import jax
import jax.numpy as jnp
import numpy as np
from jax import lax
from jax.experimental import pallas as pl
from jax.experimental.pallas import tpu as pltpu
from jax.sharding import PartitionSpec as P

BF = jnp.bfloat16
F32 = jnp.float32
VM = pltpu.VMEM
ANY = pl.ANY
MESH = pl.DeviceIdType.MESH
DMA = pltpu.SemaphoreType.DMA
BLOCK = 256
COLS = 512


def flip(index, bits):
    out = index
    bit = 1
    while bit <= bits:
        if bits & bit:
            out = out + bit - 2 * bit * lax.rem(lax.div(index, bit), 2)
        bit *= 2
    return out


def dot(a, b):
    return jnp.dot(a, b, preferred_element_type=F32)


def turn(x, cos, sin, head_dim):
    width = x.shape[1]
    half = head_dim // 2
    lane = lax.broadcasted_iota(jnp.int32, x.shape, 1)
    first = lane % head_dim < half
    other = jnp.where(first, pltpu.roll(x, width - half, 1), pltpu.roll(x, half, 1))
    reps = width // cos.shape[1]
    return x * jnp.concatenate([cos] * reps, axis=1) + other * jnp.concatenate([sin] * reps, axis=1)


class Sizes:
    def __init__(self, ep, tokens, width, top, rows, heads, dk, dv, hidden, features):
        self.ep, self.tokens, self.width, self.top = ep, tokens, width, top
        self.rows, self.heads, self.dk, self.dv = rows, heads, dk, dv
        self.hidden, self.features = hidden, features
        self.half = width // 2
        self.cap = 3 * tokens * top // (2 * ep)
        self.one = -(-2 * self.cap // 16) * 16
        self.two = 2 * self.one
        self.near = ep // 2
        self.blocks = rows // BLOCK
        self.stages = ep.bit_length() - 1


def kernel(
    z,
    q_hbm, k_hbm, v_hbm, g_hbm, decay_ref, wo_hbm, tok_hbm, gain_ref, routes_ref, rweight_ref,
    wg_hbm, wu_hbm, wd_hbm, spin_ref, base_ref,
    mixed_hbm, moe_hbm,
    q_v, k_v, v_v, g_v, wo_v, tok_v, wg_v, wu_v, wd_v,
    nh, nb, meta, sn, sc, xf, yk, ys, yr, xr, zc, rn, rc, own, fxs, fxr, fin,
    wnh, wnl, wch, wcl, pn, keyt, upd, run_v, runt_v, pack_s, pack_r, pre_v, gate_all, mix_v,
    load_sem, send_sem, recv_sem, out_sem,
):
    e = lax.axis_index("ep")
    t = lax.axis_index("tp")
    c = lax.rem(t, 2)
    o = 1 - c
    pair = (e, flip(t, 1))
    cross = (e, flip(t, 2))
    diag = (e, flip(t, 3))
    H, ONE, TWO, NEAR, TOK, CAP = z.half, z.one, z.two, z.near, z.tokens, z.cap
    used = [0]
    sent = []

    barrier = pltpu.get_barrier_semaphore()
    peers = [(flip(e, d), t) for d in range(1, z.ep)] + [pair, cross, diag]
    for peer in peers:
        pl.semaphore_signal(barrier, inc=1, device_id=peer, device_id_type=MESH)

    loads = {}

    def load(name, src, dst):
        copy = pltpu.make_async_copy(src, dst, load_sem.at[len(loads)])
        copy.start()
        loads[name] = copy

    load("tok", tok_hbm, tok_v)
    load("k", k_hbm, k_v)
    load("v", v_hbm, v_v)
    load("q", q_hbm, q_v)
    load("g", g_hbm, g_v)
    load("wg", wg_hbm.at[0], wg_v)
    load("wu", wu_hbm.at[0], wu_v)
    for h in range(2):
        load("wd%d" % h, wd_hbm.at[0, :, pl.ds(h * H, H)], wd_v.at[h])
    load("wo", wo_hbm, wo_v)

    def send(src, dst, device):
        i = used[0]
        used[0] += 1
        copy = pltpu.make_async_remote_copy(
            src_ref=src, dst_ref=dst, send_sem=send_sem.at[i], recv_sem=recv_sem.at[i],
            device_id=device, device_id_type=MESH,
        )
        copy.start()
        sent.append(copy)
        return copy

    lane = lax.broadcasted_iota(jnp.int32, (TOK, 128), 1)
    packed = jnp.zeros((TOK, 128), F32)
    for r in range(2):
        packed = packed + jnp.where(lane == r, routes_ref[:, r : r + 1].astype(F32), 0.0)
        packed = packed + jnp.where(lane == 2 + r, rweight_ref[:, r : r + 1], 0.0)
    meta[c] = packed
    pl.semaphore_wait(barrier, len(peers))
    metas = [
        send(meta.at[c], meta.at[c], pair),
        send(meta.at[c], meta.at[2 + c], cross),
        send(meta.at[c], meta.at[2 + c], diag),
    ]

    loads["tok"].wait()
    x = tok_v[...].astype(F32)
    centered = x - jnp.mean(x, axis=-1, keepdims=True)
    variance = jnp.mean(centered * centered, axis=-1, keepdims=True)
    normed = (centered * lax.rsqrt(variance + 1e-05) * gain_ref[...]).astype(BF)
    nh[0] = normed[:, :H]
    nh[1] = normed[:, H:]
    toks = [
        send(nh.at[o], nb.at[c], pair),
        send(nh.at[c], nb.at[2 + c], cross),
        send(nh.at[o], nb.at[2 + c], diag),
    ]
    nb[c] = nh[c]

    for copy in metas:
        copy.wait_recv()
    every = 4 * TOK
    info = meta[...].reshape(every, 128)
    number = lax.broadcasted_iota(jnp.int32, (every, 128), 1)
    token = lax.broadcasted_iota(jnp.int32, (every, 1), 0)
    away = lax.div(token, 2 * TOK)
    side = lax.rem(lax.div(token, TOK), 2)
    rel = [jnp.bitwise_xor(info[:, r : r + 1].astype(jnp.int32), e) for r in range(2)]
    hits = [(rel[r] == number).astype(F32) for r in range(2)]
    i = lax.broadcasted_iota(jnp.int32, (every, every), 0)
    j = lax.broadcasted_iota(jnp.int32, (every, every), 1)
    earlier = ((j < i) & (lax.div(i, TOK) == lax.div(j, TOK))).astype(F32).astype(BF)
    before = dot(earlier, (hits[0] + hits[1]).astype(BF))
    near_lane = lax.broadcasted_iota(jnp.int32, (every, NEAR * TWO), 1)
    far_lane = lax.broadcasted_iota(jnp.int32, (2 * TOK, NEAR * ONE), 1)
    near_place = jnp.zeros((every, NEAR * TWO), F32)
    near_weight = jnp.zeros((every, NEAR * TWO), F32)
    far_place = jnp.zeros((2 * TOK, NEAR * ONE), F32)
    far_weight = jnp.zeros((2 * TOK, NEAR * ONE), F32)
    for r in range(2):
        slot = jnp.sum(before * hits[r], axis=1, keepdims=True).astype(jnp.int32) + side * CAP
        weight = info[:, 2 + r : 3 + r]
        near_at = jnp.where(rel[r] < NEAR, rel[r] * TWO + away * ONE + slot, -1)
        far_at = jnp.where(rel[r] >= NEAR, (rel[r] - NEAR) * ONE + slot, -1)[: 2 * TOK]
        near_here = near_at == near_lane
        far_here = far_at == far_lane
        near_place = near_place + jnp.where(near_here, 1.0, 0.0)
        near_weight = near_weight + jnp.where(near_here, weight, 0.0)
        far_place = far_place + jnp.where(far_here, 1.0, 0.0)
        far_weight = far_weight + jnp.where(far_here, weight[: 2 * TOK], 0.0)
    for value, high, low in ((near_weight, wnh, wnl), (far_weight, wch, wcl)):
        top = value.astype(BF)
        high[...] = top
        low[...] = (value - top.astype(F32)).astype(BF)
    pn[...] = near_place.T.astype(BF)
    placing = far_place.T.astype(BF)

    toks[0].wait_recv()
    for col in range(0, H, COLS):
        rows = jnp.concatenate([nb[g, :, col : col + COLS] for g in range(2)], axis=0)
        sc[:, col : col + COLS] = dot(placing, rows).astype(BF)
    far_in = [
        send(sc.at[pl.ds(d * ONE, ONE)], xf.at[c, pl.ds((NEAR + d) * TWO, ONE)], (flip(e, NEAR + d), t))
        for d in range(NEAR)
    ]

    heads, dk, dv = z.heads, z.dk, z.dv
    size = heads * dk
    run = decay_ref[...]
    along = lax.broadcasted_iota(jnp.int32, run.shape, 1) % BLOCK
    step = 1
    while step < BLOCK:
        run = run + jnp.where(along >= step, pltpu.roll(run, step, 1), 0.0)
        step *= 2
    for b in range(z.blocks):
        part = run[:, b * BLOCK : (b + 1) * BLOCK]
        run_v[b] = part
        runt_v[b] = jnp.concatenate([part] * (8 // heads), axis=0).T

    def tables(b):
        at = e * z.blocks + b
        cos_b = base_ref[0, pl.ds(at, 1), :]
        sin_b = base_ref[1, pl.ds(at, 1), :]
        cos = cos_b * spin_ref[0] - sin_b * spin_ref[1]
        sin = sin_b * spin_ref[0] + cos_b * spin_ref[1]
        lane = lax.broadcasted_iota(jnp.int32, sin.shape, 1)
        return cos, jnp.where(lane % dk < dk // 2, -sin, sin)

    loads["k"].wait()
    loads["v"].wait()
    state = [jnp.zeros((dk, dv), F32)] * heads
    total = [jnp.zeros((1, 1), F32)] * heads
    for b in range(z.blocks):
        at = slice(b * BLOCK, (b + 1) * BLOCK)
        cos, sin = tables(b)
        kt = (turn(k_v[at, :].astype(F32), cos, sin, dk) * dk ** (-0.5)).T
        keyt[b] = kt.astype(BF)
        for h in range(heads):
            rows = slice(h * dk, (h + 1) * dk)
            run_row = run_v[b, h : h + 1, :]
            closing = run_row[:, BLOCK - 1 : BLOCK]
            scaled = (kt[rows, :] * jnp.exp(closing - run_row)).astype(BF)
            new = dot(scaled, v_v[at, h * dv : (h + 1) * dv])
            upd[b, rows, :] = new
            state[h] = state[h] * jnp.exp(closing) + new
            total[h] = total[h] + closing
    group = jnp.concatenate(state, axis=0)
    fade = jnp.concatenate([jnp.broadcast_to(jnp.exp(x), (dk, dv)) for x in total], axis=0)
    prefix = jnp.zeros((size, dv), F32)
    prefade = jnp.ones((size, dv), F32)
    scans = []

    def scan_send(s):
        pack_s[s, 0:size] = group.astype(BF)
        pack_s[s, size:] = fade.astype(BF)
        scans.append(send(pack_s.at[s], pack_r.at[s], (flip(e, 1 << s), t)))

    def scan_recv(s, group, fade, prefix, prefade):
        scans[s].wait_recv()
        other = pack_r[s, 0:size].astype(F32)
        other_fade = pack_r[s, size:].astype(F32)
        later = lax.rem(lax.div(e, 1 << s), 2) == 1
        prefix = jnp.where(later, prefix + prefade * other, prefix)
        prefade = jnp.where(later, prefade * other_fade, prefade)
        group = jnp.where(later, other * fade + group, group * other_fade + other)
        return group, fade * other_fade, prefix, prefade

    scan_send(0)

    toks[1].wait_recv()
    toks[2].wait_recv()
    for col in range(0, H, COLS):
        rows = jnp.concatenate([nb[g, :, col : col + COLS] for g in range(4)], axis=0)
        made = dot(pn[...], rows).astype(BF)
        xf[c, 0:TWO, col : col + COLS] = made[0:TWO]
        sn[:, col : col + COLS] = made[TWO:]
    near_in = [None] + [
        send(sn.at[pl.ds((d - 1) * TWO, TWO)], xf.at[c, pl.ds(d * TWO, TWO)], (flip(e, d), t))
        for d in range(1, NEAR)
    ]

    for s in range(1, z.stages):
        group, fade, prefix, prefade = scan_recv(s - 1, group, fade, prefix, prefade)
        scan_send(s)

    pairs = {}

    def to_pair(at, count):
        where = xf.at[c, pl.ds(at, count)]
        pairs[at] = send(where, where, pair)

    to_pair(0, TWO)
    far_x = {}

    def relay(d):
        far_in[d].wait_recv()
        at = (NEAR + d) * TWO
        far_x[d] = send(xf.at[c, pl.ds(at, ONE)], xf.at[c, pl.ds(at + ONE, ONE)], cross)
        to_pair(at, ONE)

    def relay_on(d):
        far_x[d].wait_recv()
        to_pair((NEAR + d) * TWO + ONE, ONE)

    def relay_near(d):
        near_in[d].wait_recv()
        to_pair(d * TWO, TWO)

    own_gate, near_gate, far_gate = [], [], []

    def mix(b, state):
        at = slice(b * BLOCK, (b + 1) * BLOCK)
        cos, sin = tables(b)
        q = turn(q_v[at, :].astype(F32), cos, sin, dk)
        row = lax.broadcasted_iota(jnp.int32, (BLOCK, BLOCK), 0)
        col = lax.broadcasted_iota(jnp.int32, (BLOCK, BLOCK), 1)
        causal = row >= col
        after = []
        for h in range(heads):
            rows = slice(h * dk, (h + 1) * dk)
            run_row = run_v[b, h : h + 1, :]
            run_col = runt_v[b, :, h : h + 1]
            closing = run_row[:, BLOCK - 1 : BLOCK]
            qh = q[:, rows]
            vh = v_v[at, h * dv : (h + 1) * dv]
            weights = jnp.where(causal, jnp.exp(jnp.where(causal, run_col - run_row, 0.0)), 0.0)
            scores = dot(qh.astype(BF), keyt[b, rows, :]) * weights
            out = dot(scores.astype(BF), vh)
            carried = state[rows, :]
            out = out + dot((qh * jnp.exp(run_col)).astype(BF), carried.astype(BF))
            after.append(carried * jnp.exp(closing) + upd[b, rows, :])
            centered = out - jnp.mean(out, axis=-1, keepdims=True)
            variance = jnp.mean(centered * centered, axis=-1, keepdims=True)
            gate = g_v[at, h * dv : (h + 1) * dv].astype(F32)
            act = gate / (1.0 + jnp.exp(-gate))
            gate_all[0, at, h * dv : (h + 1) * dv] = (act * (centered * lax.rsqrt(variance + 1e-06))).astype(BF)
        return jnp.concatenate(after, axis=0)

    def gate_x(b):
        at = pl.ds(b * BLOCK, BLOCK)
        far_gate.append(send(gate_all.at[0, at], gate_all.at[2, at], cross))
        near_gate.append(send(gate_all.at[0, at], gate_all.at[1, at], pair))

    last_gate = []

    def gate_on(b):
        far_gate[b].wait_recv()
        at = pl.ds(b * BLOCK, BLOCK)
        last_gate.append(send(gate_all.at[2, at], gate_all.at[3, at], pair))

    stores = []

    def project(b):
        near_gate[b].wait_recv()
        last_gate[b].wait_recv()
        at = slice(b * BLOCK, (b + 1) * BLOCK)
        sum_ = dot(gate_all[0, at], wo_v[t])
        for g in range(1, 4):
            sum_ = sum_ + dot(gate_all[g, at], wo_v[flip(t, g)])
        mix_v[at, :] = sum_.astype(BF)
        at = pl.ds(b * BLOCK, BLOCK)
        copy = pltpu.make_async_copy(mix_v.at[at], mixed_hbm.at[at], out_sem.at[len(stores)])
        copy.start()
        stores.append(copy)

    quarter = z.ep // 4
    trade = {}

    def ffn(part):
        at = part * quarter * TWO
        count = quarter * TWO
        rows = slice(at, at + count)
        gate = dot(xf[0, rows], wg_v[0:H]) + dot(xf[1, rows], wg_v[H:])
        up = dot(xf[0, rows], wu_v[0:H]) + dot(xf[1, rows], wu_v[H:])
        hidden = (gate * up / (1.0 + jnp.exp(-gate))).astype(BF)
        ys[rows] = dot(hidden, wd_v[o]).astype(BF)
        where = pl.ds(at, count)
        trade[part] = send(ys.at[where], yr.at[where], pair)
        yk[rows] = dot(hidden, wd_v[c]).astype(BF)

    def wait_pairs(part):
        for d in range(part * quarter, (part + 1) * quarter):
            pairs[d * TWO].wait_recv()
            if d >= NEAR:
                pairs[d * TWO + ONE].wait_recv()

    def core_sum(part):
        trade[part].wait_recv()
        at = part * quarter * TWO
        rows = slice(at, at + quarter * TWO)
        yk[rows] = (yk[rows].astype(F32) + yr[rows].astype(F32)).astype(BF)

    near_out, far_sum, far_out = {}, {}, {}

    def near_back(part):
        core_sum(part)
        for d in range(part * quarter, (part + 1) * quarter):
            if d:
                at = pl.ds(d * TWO, TWO)
                near_out[d] = send(yk.at[at], rn.at[pl.ds((d - 1) * TWO, TWO)], (flip(e, d), t))

    def far_back(part):
        core_sum(part)
        for d in range(part * quarter - NEAR, (part + 1) * quarter - NEAR):
            at = (NEAR + d) * TWO + ONE
            far_sum[d] = send(yk.at[pl.ds(at, ONE)], xr.at[pl.ds(d * ONE, ONE)], cross)

    def far_home(part):
        for d in range(part * quarter - NEAR, (part + 1) * quarter - NEAR):
            far_sum[d].wait_recv()
            at = (NEAR + d) * TWO
            rows = slice(d * ONE, (d + 1) * ONE)
            zc[rows] = (yk[at : at + ONE].astype(F32) + xr[rows].astype(F32)).astype(BF)
            far_out[d] = send(zc.at[pl.ds(d * ONE, ONE)], rc.at[pl.ds(d * ONE, ONE)], (flip(e, NEAR + d), t))

    first = list(range(quarter))
    second = list(range(quarter, NEAR))
    front, back = first[: len(first) // 2], first[len(first) // 2 :]
    for d in front:
        relay(d)
    group, fade, prefix, prefade = scan_recv(z.stages - 1, group, fade, prefix, prefade)
    loads["q"].wait()
    loads["g"].wait()
    state = mix(0, prefix)
    for d in back:
        relay(d)
    gate_x(0)
    state = mix(1, state)
    for d in first:
        relay_on(d)
    for name in ("wg", "wu", "wd0", "wd1"):
        loads[name].wait()
    wait_pairs(2)
    ffn(2)
    for d in range(1, quarter):
        relay_near(d)
    far_back(2)
    gate_x(1)
    front, back = second[: len(second) // 2], second[len(second) // 2 :]
    for d in front:
        relay(d)
    wait_pairs(0)
    ffn(0)
    for d in range(quarter, NEAR):
        relay_near(d)
    far_home(2)
    near_back(0)
    wait_pairs(1)
    ffn(1)
    state = mix(2, state)
    near_back(1)
    for d in back:
        relay(d)
    gate_x(2)
    mix(3, state)
    for d in second:
        relay_on(d)
    wait_pairs(3)
    ffn(3)
    far_back(3)
    gate_x(3)
    loads["wo"].wait()
    gate_on(0)
    gate_on(1)
    project(0)
    far_home(3)
    gate_on(2)
    project(1)
    project(2)

    for d in range(1, NEAR):
        near_out[d].wait_recv()
    for col in range(0, H, COLS):
        at = slice(col, col + COLS)
        total = dot(wnh[:, 0:TWO], yk[0:TWO, at]) + dot(wnl[:, 0:TWO], yk[0:TWO, at])
        total = total + dot(wnh[:, TWO:], rn[:, at]) + dot(wnl[:, TWO:], rn[:, at])
        own[:, at] = total[: 2 * TOK]
        fxs[:, at] = total[2 * TOK :].astype(BF)
    last = send(fxs, fxr, cross)
    gate_on(3)
    project(3)
    for d in range(NEAR):
        far_out[d].wait_recv()
    last.wait_recv()
    for col in range(0, H, COLS):
        at = slice(col, col + COLS)
        total = dot(wch[...], rc[:, at]) + dot(wcl[...], rc[:, at])
        total = total + own[:, at] + fxr[:, at].astype(F32)
        fin[0, :, at] = total[:TOK].astype(BF)
        fin[1, :, at] = total[TOK:].astype(BF)
    mine = pl.ds(pl.multiple_of(c * H, H), H)
    done = send(fin.at[o], moe_hbm.at[:, mine], pair)
    copy = pltpu.make_async_copy(fin.at[c], moe_hbm.at[:, mine], out_sem.at[len(stores)])
    copy.start()
    stores.append(copy)
    done.wait_recv()
    for copy in stores:
        copy.wait()
    for copy in sent:
        copy.wait_send()


def copies(z):
    return 6 + z.near * 2 + z.stages + z.near * 3 + 3 * z.blocks + 4 + 3 * z.near + 8


def per_device(
    query, keys, values, gate_pre, log_decay, out_weight, expert_input, norm_gain, routes,
    route_weights, w_gate, w_up, w_down,
):
    rows, heads = query.shape[0], log_decay.shape[0]
    dk, dv = query.shape[1] // heads, values.shape[1] // heads
    tokens, width = expert_input.shape
    hidden, features = w_gate.shape[2], out_weight.shape[1]
    ep, tp = lax.axis_size("ep"), lax.axis_size("tp")
    z = Sizes(ep, tokens, width, routes.shape[1], rows, heads, dk, dv, hidden, features)
    inverse = (1.0 / 10000.0 ** np.linspace(0.0, 1.0, dk // 2)).astype(np.float32).astype(np.float64)
    inverse = np.tile(inverse, 128 // (dk // 2))
    spin = np.arange(BLOCK)[:, None] * inverse[None, :]
    base = (np.arange(ep * z.blocks) * BLOCK)[:, None] * inverse[None, :]
    spin = jnp.asarray(np.stack([np.cos(spin), np.sin(spin)]).astype(np.float32))
    base = jnp.asarray(np.stack([np.cos(base), np.sin(base)]).astype(np.float32))
    H, ONE, TWO, NEAR = z.half, z.one, z.two, z.near
    size = heads * dk
    depth = heads * dv
    inside = pl.BlockSpec(memory_space=VM)
    outside = pl.BlockSpec(memory_space=ANY)
    scratch = [
        VM((rows, size), BF), VM((rows, size), BF), VM((rows, depth), BF), VM((rows, depth), BF),
        VM((tp, depth, features), BF), VM((tokens, width), BF),
        VM((width, hidden), BF), VM((width, hidden), BF), VM((2, hidden, H), BF),
        VM((2, tokens, H), BF), VM((4, tokens, H), BF), VM((4, tokens, 128), F32),
        VM(((NEAR - 1) * TWO, H), BF), VM((NEAR * ONE, H), BF), VM((2, ep * TWO, H), BF),
        VM((ep * TWO, H), BF), VM((ep * TWO, H), BF), VM((ep * TWO, H), BF),
        VM((NEAR * ONE, H), BF), VM((NEAR * ONE, H), BF),
        VM(((NEAR - 1) * TWO, H), BF), VM((NEAR * ONE, H), BF),
        VM((2 * tokens, H), F32), VM((2 * tokens, H), BF), VM((2 * tokens, H), BF), VM((2, tokens, H), BF),
        VM((4 * tokens, NEAR * TWO), BF), VM((4 * tokens, NEAR * TWO), BF),
        VM((2 * tokens, NEAR * ONE), BF), VM((2 * tokens, NEAR * ONE), BF),
        VM((NEAR * TWO, 4 * tokens), BF),
        VM((z.blocks, size, BLOCK), BF), VM((z.blocks, size, dv), F32),
        VM((z.blocks, heads, BLOCK), F32), VM((z.blocks, BLOCK, 8), F32),
        VM((z.stages, 2 * size, dv), BF), VM((z.stages, 2 * size, dv), BF), VM((size, dv), F32),
        VM((4, rows, depth), BF), VM((rows, features), BF),
        DMA((10,)), DMA((copies(z),)), DMA((copies(z),)), DMA((z.blocks + 1,)),
    ]
    return pl.pallas_call(
        functools.partial(kernel, z),
        in_specs=[outside] * 4 + [inside, outside, outside] + [inside] * 3 + [outside] * 3 + [inside] * 2,
        out_specs=[outside, outside],
        out_shape=[
            jax.ShapeDtypeStruct((rows, features), BF),
            jax.ShapeDtypeStruct((tokens, width), BF),
        ],
        scratch_shapes=scratch,
        compiler_params=pltpu.CompilerParams(
            collective_id=0, has_side_effects=True, vmem_limit_bytes=67043328
        ),
        cost_estimate=pl.CostEstimate(flops=10**10, bytes_accessed=20 << 20, transcendentals=0),
    )(
        query, keys, values, gate_pre, log_decay, out_weight.reshape(tp, depth, features), expert_input,
        norm_gain.reshape(1, width), routes, route_weights, w_gate, w_up, w_down, spin, base,
    )


def solution(mesh):
    placed = (
        P("ep", "tp"),
        P("ep", "tp"),
        P("ep", "tp"),
        P("ep", "tp"),
        P("tp", "ep"),
        P(None, "tp"),
        P(("ep", "tp"), None),
        P(),
        P(("ep", "tp"), None),
        P(("ep", "tp"), None),
        P("ep", None, "tp"),
        P("ep", None, "tp"),
        P("ep", "tp", None),
    )
    return jax.shard_map(
        per_device,
        mesh=mesh,
        in_specs=placed,
        out_specs=(P("ep", "tp"), P(("ep", "tp"), None)),
        check_vma=False,
    )
```

profile of v0, /device:TPU:0, one launch (start us, length us, event | category | flops | bytes accessed | tf_op | source)
XLA Modules:
  0.0 152.1 jit_solution(11821431430064515477)
XLA Ops:
  0.6 1.4 copy.17.routes_ref
  2.0 1.4 copy.18.rweight_ref
  3.4 144.7 %shard_map.158 = (bf16[1024,1024]{1,0:T(8,128)(2,1)}, bf16[64,4096]{1,0:T(8,128)(2,1)}) custom-call(bf16[1024,256]{1,0:T(8,128)(2,1)} %q_hbm.1, bf16[1024,256]{1,0:T(8,128)(2,1)} %k_hbm.1, bf16[1024,512]{1,0:T(8,128)(2,1)} %v_hbm.1, bf16[1024,512]{1,0:T(8,128)(2,1)} %g_hbm.1, f32[4,1024]{1,0:T(4,128)} %decay_ref.1, bf16[4,512,1024]{2,1,0:T(8,128)(2,1)} %bitcast.2, ...), custom_call_target="tpu_custom_call" | custom-call | flops 10000000000 | bytes 20971520 | tf_op jit(solution)/shard_map/pallas_call | solution.py:527
  148.1 0.0 copy-start
  148.2 3.1 %copy.21 = bf16[1024,1024]{1,0:T(8,128)(2,1)} copy(bf16[1024,1024]{1,0:T(8,128)(2,1)} %get-tuple-element.4) | data formatting | bytes 4194304
  151.3 0.0 copy-done
  151.3 0.8 copy.22
Async XLA Ops:
  148.1 3.1 %copy-start = (bf16[64,4096]{1,0:T(8,128)(2,1)S(1)}, bf16[64,4096]{1,0:T(8,128)(2,1)}, u32[]{:S(2)}) copy-start(bf16[64,4096]{1,0:T(8,128)(2,1)} %get-tuple-element.5) | copy-start | bytes 1572868
where the time goes:
time: 152 us
  Pallas kernels  145 us (95%)
  local copies, waits for them, and re-layouts  6.7 us (4%)
    pallas_call x1, Pallas kernels, per_device(): pl.pallas_call(functools.partial(kernel, z), in_specs=[outside] * 4 + [in...  145 us
    unnamed x6, local copies, waits for them, and re-layouts  6.7 us

commit v1 on v0

--- a/solution.py
+++ b/solution.py
@@ -25,6 +25,9 @@
             out = out + bit - 2 * bit * lax.rem(lax.div(index, bit), 2)
         bit *= 2
     return out
+
+
+phase = jax.named_scope
 
 
 def dot(a, b):
@@ -61,8 +64,8 @@
     wg_hbm, wu_hbm, wd_hbm, spin_ref, base_ref,
     mixed_hbm, moe_hbm,
     q_v, k_v, v_v, g_v, wo_v, tok_v, wg_v, wu_v, wd_v,
-    nh, nb, meta, sn, sc, xf, yk, ys, yr, xr, zc, rn, rc, own, fxs, fxr, fin,
-    wnh, wnl, wch, wcl, pn, keyt, upd, run_v, runt_v, pack_s, pack_r, pre_v, gate_all, mix_v,
+    nh, nb, meta, sn, sc, xf, yk, ys, yr, xr, zc, rc, fin,
+    wch, wcl, pn, keyt, upd, run_v, runt_v, pack_s, pack_r, pre_v, gate_all, mix_v,
     load_sem, send_sem, recv_sem, out_sem,
 ):
     e = lax.axis_index("ep")
@@ -110,80 +113,17 @@
         sent.append(copy)
         return copy
 
-    lane = lax.broadcasted_iota(jnp.int32, (TOK, 128), 1)
-    packed = jnp.zeros((TOK, 128), F32)
-    for r in range(2):
-        packed = packed + jnp.where(lane == r, routes_ref[:, r : r + 1].astype(F32), 0.0)
-        packed = packed + jnp.where(lane == 2 + r, rweight_ref[:, r : r + 1], 0.0)
-    meta[c] = packed
-    pl.semaphore_wait(barrier, len(peers))
-    metas = [
-        send(meta.at[c], meta.at[c], pair),
-        send(meta.at[c], meta.at[2 + c], cross),
-        send(meta.at[c], meta.at[2 + c], diag),
-    ]
-
-    loads["tok"].wait()
+    both = jnp.concatenate([routes_ref[...].astype(F32), rweight_ref[...]], axis=0)
+    meta[c] = jnp.concatenate([both] * (8 // both.shape[0]), axis=0)
+
+    with phase("wait_tok"):
+        loads["tok"].wait()
     x = tok_v[...].astype(F32)
     centered = x - jnp.mean(x, axis=-1, keepdims=True)
     variance = jnp.mean(centered * centered, axis=-1, keepdims=True)
     normed = (centered * lax.rsqrt(variance + 1e-05) * gain_ref[...]).astype(BF)
     nh[0] = normed[:, :H]
     nh[1] = normed[:, H:]
-    toks = [
-        send(nh.at[o], nb.at[c], pair),
-        send(nh.at[c], nb.at[2 + c], cross),
-        send(nh.at[o], nb.at[2 + c], diag),
-    ]
-    nb[c] = nh[c]
-
-    for copy in metas:
-        copy.wait_recv()
-    every = 4 * TOK
-    info = meta[...].reshape(every, 128)
-    number = lax.broadcasted_iota(jnp.int32, (every, 128), 1)
-    token = lax.broadcasted_iota(jnp.int32, (every, 1), 0)
-    away = lax.div(token, 2 * TOK)
-    side = lax.rem(lax.div(token, TOK), 2)
-    rel = [jnp.bitwise_xor(info[:, r : r + 1].astype(jnp.int32), e) for r in range(2)]
-    hits = [(rel[r] == number).astype(F32) for r in range(2)]
-    i = lax.broadcasted_iota(jnp.int32, (every, every), 0)
-    j = lax.broadcasted_iota(jnp.int32, (every, every), 1)
-    earlier = ((j < i) & (lax.div(i, TOK) == lax.div(j, TOK))).astype(F32).astype(BF)
-    before = dot(earlier, (hits[0] + hits[1]).astype(BF))
-    near_lane = lax.broadcasted_iota(jnp.int32, (every, NEAR * TWO), 1)
-    far_lane = lax.broadcasted_iota(jnp.int32, (2 * TOK, NEAR * ONE), 1)
-    near_place = jnp.zeros((every, NEAR * TWO), F32)
-    near_weight = jnp.zeros((every, NEAR * TWO), F32)
-    far_place = jnp.zeros((2 * TOK, NEAR * ONE), F32)
-    far_weight = jnp.zeros((2 * TOK, NEAR * ONE), F32)
-    for r in range(2):
-        slot = jnp.sum(before * hits[r], axis=1, keepdims=True).astype(jnp.int32) + side * CAP
-        weight = info[:, 2 + r : 3 + r]
-        near_at = jnp.where(rel[r] < NEAR, rel[r] * TWO + away * ONE + slot, -1)
-        far_at = jnp.where(rel[r] >= NEAR, (rel[r] - NEAR) * ONE + slot, -1)[: 2 * TOK]
-        near_here = near_at == near_lane
-        far_here = far_at == far_lane
-        near_place = near_place + jnp.where(near_here, 1.0, 0.0)
-        near_weight = near_weight + jnp.where(near_here, weight, 0.0)
-        far_place = far_place + jnp.where(far_here, 1.0, 0.0)
-        far_weight = far_weight + jnp.where(far_here, weight[: 2 * TOK], 0.0)
-    for value, high, low in ((near_weight, wnh, wnl), (far_weight, wch, wcl)):
-        top = value.astype(BF)
-        high[...] = top
-        low[...] = (value - top.astype(F32)).astype(BF)
-    pn[...] = near_place.T.astype(BF)
-    placing = far_place.T.astype(BF)
-
-    toks[0].wait_recv()
-    for col in range(0, H, COLS):
-        rows = jnp.concatenate([nb[g, :, col : col + COLS] for g in range(2)], axis=0)
-        sc[:, col : col + COLS] = dot(placing, rows).astype(BF)
-    far_in = [
-        send(sc.at[pl.ds(d * ONE, ONE)], xf.at[c, pl.ds((NEAR + d) * TWO, ONE)], (flip(e, NEAR + d), t))
-        for d in range(NEAR)
-    ]
-
     heads, dk, dv = z.heads, z.dk, z.dv
     size = heads * dk
     run = decay_ref[...]
@@ -225,40 +165,103 @@
             state[h] = state[h] * jnp.exp(closing) + new
             total[h] = total[h] + closing
     group = jnp.concatenate(state, axis=0)
-    fade = jnp.concatenate([jnp.broadcast_to(jnp.exp(x), (dk, dv)) for x in total], axis=0)
+    fade = [jnp.broadcast_to(jnp.exp(x), (1, dv)) for x in total]
     prefix = jnp.zeros((size, dv), F32)
     prefade = jnp.ones((size, dv), F32)
     scans = []
 
+    def spread(fade):
+        return jnp.concatenate([jnp.broadcast_to(x, (dk, dv)) for x in fade], axis=0)
+
+    @phase("scan_send")
     def scan_send(s):
         pack_s[s, 0:size] = group.astype(BF)
-        pack_s[s, size:] = fade.astype(BF)
+        pack_s[s, size:] = jnp.concatenate(fade * (16 // heads), axis=0).astype(BF)
         scans.append(send(pack_s.at[s], pack_r.at[s], (flip(e, 1 << s), t)))
 
+    @phase("scan_recv")
     def scan_recv(s, group, fade, prefix, prefade):
         scans[s].wait_recv()
         other = pack_r[s, 0:size].astype(F32)
-        other_fade = pack_r[s, size:].astype(F32)
+        rows = pack_r[s, size:].astype(F32)
+        other_fade = [rows[h : h + 1] for h in range(heads)]
+        all_fade = spread(other_fade)
         later = lax.rem(lax.div(e, 1 << s), 2) == 1
         prefix = jnp.where(later, prefix + prefade * other, prefix)
-        prefade = jnp.where(later, prefade * other_fade, prefade)
-        group = jnp.where(later, other * fade + group, group * other_fade + other)
-        return group, fade * other_fade, prefix, prefade
-
+        prefade = jnp.where(later, prefade * all_fade, prefade)
+        group = jnp.where(later, other * spread(fade) + group, group * all_fade + other)
+        return group, [a * b for a, b in zip(fade, other_fade)], prefix, prefade
+
+    with phase("barrier"):
+        pl.semaphore_wait(barrier, len(peers))
+    metas = [
+        send(meta.at[c], meta.at[c], pair),
+        send(meta.at[c], meta.at[2 + c], cross),
+        send(meta.at[c], meta.at[2 + c], diag),
+    ]
+    toks = [
+        send(nh.at[o], nb.at[c], pair),
+        send(nh.at[c], nb.at[2 + c], cross),
+        send(nh.at[o], nb.at[2 + c], diag),
+    ]
     scan_send(0)
-
-    toks[1].wait_recv()
-    toks[2].wait_recv()
+    nb[c] = nh[c]
+
+
+    with phase("wait_metas"):
+        for copy in metas:
+            copy.wait_recv()
+    every = 4 * TOK
+    info = jnp.concatenate([meta[g].T for g in range(4)], axis=0)
+    number = lax.broadcasted_iota(jnp.int32, (every, 128), 1)
+    token = lax.broadcasted_iota(jnp.int32, (every, 1), 0)
+    away = lax.div(token, 2 * TOK)
+    side = lax.rem(lax.div(token, TOK), 2)
+    rel = [jnp.bitwise_xor(info[:, r : r + 1].astype(jnp.int32), e) for r in range(2)]
+    hits = [(rel[r] == number).astype(F32) for r in range(2)]
+    i = lax.broadcasted_iota(jnp.int32, (every, every), 0)
+    j = lax.broadcasted_iota(jnp.int32, (every, every), 1)
+    earlier = ((j < i) & (lax.div(i, TOK) == lax.div(j, TOK))).astype(F32).astype(BF)
+    before = dot(earlier, (hits[0] + hits[1]).astype(BF))
+    near_lane = lax.broadcasted_iota(jnp.int32, (every, NEAR * TWO), 1)
+    far_lane = lax.broadcasted_iota(jnp.int32, (2 * TOK, NEAR * ONE), 1)
+    near_place = jnp.zeros((every, NEAR * TWO), F32)
+    far_place = jnp.zeros((2 * TOK, NEAR * ONE), F32)
+    all_lane = lax.broadcasted_iota(jnp.int32, (2 * TOK, z.ep * ONE), 1)
+    all_weight = jnp.zeros((2 * TOK, z.ep * ONE), F32)
+    for r in range(2):
+        slot = jnp.sum(before * hits[r], axis=1, keepdims=True).astype(jnp.int32) + side * CAP
+        weight = info[: 2 * TOK, 2 + r : 3 + r]
+        near_at = jnp.where(rel[r] < NEAR, rel[r] * TWO + away * ONE + slot, -1)
+        far_at = jnp.where(rel[r] >= NEAR, (rel[r] - NEAR) * ONE + slot, -1)[: 2 * TOK]
+        near_here = near_at == near_lane
+        far_here = far_at == far_lane
+        near_place = near_place + jnp.where(near_here, 1.0, 0.0)
+        all_at = (rel[r] * ONE + slot)[: 2 * TOK]
+        all_weight = all_weight + jnp.where(all_at == all_lane, weight, 0.0)
+        far_place = far_place + jnp.where(far_here, 1.0, 0.0)
+    top = all_weight.astype(BF)
+    wch[...] = top
+    wcl[...] = (all_weight - top.astype(F32)).astype(BF)
+    pn[...] = near_place.T.astype(BF)
+    placing = far_place.T.astype(BF)
+
+    with phase("wait_pair_tok"):
+        toks[0].wait_recv()
     for col in range(0, H, COLS):
-        rows = jnp.concatenate([nb[g, :, col : col + COLS] for g in range(4)], axis=0)
-        made = dot(pn[...], rows).astype(BF)
-        xf[c, 0:TWO, col : col + COLS] = made[0:TWO]
-        sn[:, col : col + COLS] = made[TWO:]
-    near_in = [None] + [
-        send(sn.at[pl.ds((d - 1) * TWO, TWO)], xf.at[c, pl.ds(d * TWO, TWO)], (flip(e, d), t))
-        for d in range(1, NEAR)
-    ]
-
+        rows = jnp.concatenate([nb[g, :, col : col + COLS] for g in range(2)], axis=0)
+        sc[:, col : col + COLS] = dot(placing, rows).astype(BF)
+    far_in = {}
+
+    def far_send(d):
+        far_in[d] = send(
+            sc.at[pl.ds(d * ONE, ONE)], xf.at[c, pl.ds((NEAR + d) * TWO, ONE)], (flip(e, NEAR + d), t)
+        )
+
+    quarter = z.ep // 4
+    first = list(range(quarter))
+    second = list(range(quarter, NEAR))
+    cut = max(1, quarter // 2)
     for s in range(1, z.stages):
         group, fade, prefix, prefade = scan_recv(s - 1, group, fade, prefix, prefade)
         scan_send(s)
@@ -269,25 +272,28 @@
         where = xf.at[c, pl.ds(at, count)]
         pairs[at] = send(where, where, pair)
 
-    to_pair(0, TWO)
     far_x = {}
 
+    @phase("relay")
     def relay(d):
         far_in[d].wait_recv()
         at = (NEAR + d) * TWO
         far_x[d] = send(xf.at[c, pl.ds(at, ONE)], xf.at[c, pl.ds(at + ONE, ONE)], cross)
         to_pair(at, ONE)
 
+    @phase("relay_on")
     def relay_on(d):
         far_x[d].wait_recv()
         to_pair((NEAR + d) * TWO + ONE, ONE)
 
+    @phase("relay_near")
     def relay_near(d):
         near_in[d].wait_recv()
         to_pair(d * TWO, TWO)
 
     own_gate, near_gate, far_gate = [], [], []
 
+    @phase("mix")
     def mix(b, state):
         at = slice(b * BLOCK, (b + 1) * BLOCK)
         cos, sin = tables(b)
@@ -316,6 +322,7 @@
             gate_all[0, at, h * dv : (h + 1) * dv] = (act * (centered * lax.rsqrt(variance + 1e-06))).astype(BF)
         return jnp.concatenate(after, axis=0)
 
+    @phase("gate_x")
     def gate_x(b):
         at = pl.ds(b * BLOCK, BLOCK)
         far_gate.append(send(gate_all.at[0, at], gate_all.at[2, at], cross))
@@ -323,6 +330,7 @@
 
     last_gate = []
 
+    @phase("gate_on")
     def gate_on(b):
         far_gate[b].wait_recv()
         at = pl.ds(b * BLOCK, BLOCK)
@@ -330,6 +338,7 @@
 
     stores = []
 
+    @phase("project")
     def project(b):
         near_gate[b].wait_recv()
         last_gate[b].wait_recv()
@@ -343,9 +352,9 @@
         copy.start()
         stores.append(copy)
 
-    quarter = z.ep // 4
     trade = {}
 
+    @phase("ffn")
     def ffn(part):
         at = part * quarter * TWO
         count = quarter * TWO
@@ -358,114 +367,120 @@
         trade[part] = send(ys.at[where], yr.at[where], pair)
         yk[rows] = dot(hidden, wd_v[c]).astype(BF)
 
+    @phase("wait_pairs")
     def wait_pairs(part):
         for d in range(part * quarter, (part + 1) * quarter):
             pairs[d * TWO].wait_recv()
             if d >= NEAR:
                 pairs[d * TWO + ONE].wait_recv()
 
+    @phase("core_sum")
     def core_sum(part):
         trade[part].wait_recv()
         at = part * quarter * TWO
         rows = slice(at, at + quarter * TWO)
         yk[rows] = (yk[rows].astype(F32) + yr[rows].astype(F32)).astype(BF)
 
-    near_out, far_sum, far_out = {}, {}, {}
-
-    def near_back(part):
+    cross_sum, home_out = {}, {}
+
+    @phase("back")
+    def back(part):
         core_sum(part)
         for d in range(part * quarter, (part + 1) * quarter):
-            if d:
-                at = pl.ds(d * TWO, TWO)
-                near_out[d] = send(yk.at[at], rn.at[pl.ds((d - 1) * TWO, TWO)], (flip(e, d), t))
-
-    def far_back(part):
-        core_sum(part)
-        for d in range(part * quarter - NEAR, (part + 1) * quarter - NEAR):
-            at = (NEAR + d) * TWO + ONE
-            far_sum[d] = send(yk.at[pl.ds(at, ONE)], xr.at[pl.ds(d * ONE, ONE)], cross)
-
-    def far_home(part):
-        for d in range(part * quarter - NEAR, (part + 1) * quarter - NEAR):
-            far_sum[d].wait_recv()
-            at = (NEAR + d) * TWO
+            cross_sum[d] = send(yk.at[pl.ds(d * TWO + ONE, ONE)], xr.at[pl.ds(d * ONE, ONE)], cross)
+
+    @phase("home")
+    def home(part):
+        for d in range(part * quarter, (part + 1) * quarter):
+            cross_sum[d].wait_recv()
             rows = slice(d * ONE, (d + 1) * ONE)
-            zc[rows] = (yk[at : at + ONE].astype(F32) + xr[rows].astype(F32)).astype(BF)
-            far_out[d] = send(zc.at[pl.ds(d * ONE, ONE)], rc.at[pl.ds(d * ONE, ONE)], (flip(e, NEAR + d), t))
-
-    first = list(range(quarter))
-    second = list(range(quarter, NEAR))
-    front, back = first[: len(first) // 2], first[len(first) // 2 :]
-    for d in front:
+            full = (yk[d * TWO : d * TWO + ONE].astype(F32) + xr[rows].astype(F32)).astype(BF)
+            if d == 0:
+                rc[rows] = full
+            else:
+                zc[rows] = full
+                home_out[d] = send(zc.at[pl.ds(d * ONE, ONE)], rc.at[pl.ds(d * ONE, ONE)], (flip(e, d), t))
+
+    group, fade, prefix, prefade = scan_recv(z.stages - 1, group, fade, prefix, prefade)
+    for d in first:
+        far_send(d)
+    with phase("wait_qg"):
+        loads["q"].wait()
+        loads["g"].wait()
+    state = mix(0, prefix)
+    gate_x(0)
+
+    with phase("wait_x_tok"):
+        toks[1].wait_recv()
+        toks[2].wait_recv()
+    for col in range(0, H, COLS):
+        rows = jnp.concatenate([nb[g, :, col : col + COLS] for g in range(4)], axis=0)
+        made = dot(pn[...], rows).astype(BF)
+        xf[c, 0:TWO, col : col + COLS] = made[0:TWO]
+        sn[:, col : col + COLS] = made[TWO:]
+    near_in = {}
+    for d in range(1, NEAR):
+        near_in[d] = send(sn.at[pl.ds((d - 1) * TWO, TWO)], xf.at[c, pl.ds(d * TWO, TWO)], (flip(e, d), t))
+        if d == NEAR - 2:
+            for i in second[:cut]:
+                far_send(i)
+    for i in second[cut:]:
+        far_send(i)
+    to_pair(0, TWO)
+
+    state = mix(1, state)
+    gate_x(1)
+    state = mix(2, state)
+    for d in first[:cut]:
         relay(d)
-    group, fade, prefix, prefade = scan_recv(z.stages - 1, group, fade, prefix, prefade)
-    loads["q"].wait()
-    loads["g"].wait()
-    state = mix(0, prefix)
-    for d in back:
+    mix(3, state)
+    with phase("wait_w"):
+        for name in ("wg", "wu", "wd0", "wd1"):
+            loads[name].wait()
+    for d in first[cut:]:
         relay(d)
-    gate_x(0)
-    state = mix(1, state)
+    gate_x(2)
     for d in first:
         relay_on(d)
-    for name in ("wg", "wu", "wd0", "wd1"):
-        loads[name].wait()
     wait_pairs(2)
     ffn(2)
     for d in range(1, quarter):
         relay_near(d)
-    far_back(2)
-    gate_x(1)
-    front, back = second[: len(second) // 2], second[len(second) // 2 :]
-    for d in front:
-        relay(d)
+    back(2)
     wait_pairs(0)
     ffn(0)
+    for d in second:
+        relay(d)
     for d in range(quarter, NEAR):
         relay_near(d)
-    far_home(2)
-    near_back(0)
-    wait_pairs(1)
-    ffn(1)
-    state = mix(2, state)
-    near_back(1)
-    for d in back:
-        relay(d)
-    gate_x(2)
-    mix(3, state)
+    home(2)
+    back(0)
     for d in second:
         relay_on(d)
     wait_pairs(3)
     ffn(3)
-    far_back(3)
+    wait_pairs(1)
+    ffn(1)
+    back(3)
+    back(1)
     gate_x(3)
-    loads["wo"].wait()
-    gate_on(0)
-    gate_on(1)
+    home(0)
+    with phase("wait_wo"):
+        loads["wo"].wait()
+    for b in range(3):
+        gate_on(b)
     project(0)
-    far_home(3)
-    gate_on(2)
+    home(3)
     project(1)
+    home(1)
     project(2)
 
-    for d in range(1, NEAR):
-        near_out[d].wait_recv()
-    for col in range(0, H, COLS):
-        at = slice(col, col + COLS)
-        total = dot(wnh[:, 0:TWO], yk[0:TWO, at]) + dot(wnl[:, 0:TWO], yk[0:TWO, at])
-        total = total + dot(wnh[:, TWO:], rn[:, at]) + dot(wnl[:, TWO:], rn[:, at])
-        own[:, at] = total[: 2 * TOK]
-        fxs[:, at] = total[2 * TOK :].astype(BF)
-    last = send(fxs, fxr, cross)
-    gate_on(3)
-    project(3)
-    for d in range(NEAR):
-        far_out[d].wait_recv()
-    last.wait_recv()
+    with phase("wait_home"):
+        for d in range(1, z.ep):
+            home_out[d].wait_recv()
     for col in range(0, H, COLS):
         at = slice(col, col + COLS)
         total = dot(wch[...], rc[:, at]) + dot(wcl[...], rc[:, at])
-        total = total + own[:, at] + fxr[:, at].astype(F32)
         fin[0, :, at] = total[:TOK].astype(BF)
         fin[1, :, at] = total[TOK:].astype(BF)
     mine = pl.ds(pl.multiple_of(c * H, H), H)
@@ -473,15 +488,20 @@
     copy = pltpu.make_async_copy(fin.at[c], moe_hbm.at[:, mine], out_sem.at[len(stores)])
     copy.start()
     stores.append(copy)
-    done.wait_recv()
-    for copy in stores:
-        copy.wait()
-    for copy in sent:
-        copy.wait_send()
+    gate_on(3)
+    project(3)
+    with phase("wait_done"):
+        done.wait_recv()
+    with phase("wait_stores"):
+        for copy in stores:
+            copy.wait()
+    with phase("wait_sent"):
+        for copy in sent:
+            copy.wait_send()
 
 
 def copies(z):
-    return 6 + z.near * 2 + z.stages + z.near * 3 + 3 * z.blocks + 4 + 3 * z.near + 8
+    return 6 + z.near + (z.near - 1) + z.stages + z.near * 4 + 3 * z.blocks + 4 + 2 * z.ep
 
 
 def per_device(
@@ -509,18 +529,15 @@
         VM((rows, size), BF), VM((rows, size), BF), VM((rows, depth), BF), VM((rows, depth), BF),
         VM((tp, depth, features), BF), VM((tokens, width), BF),
         VM((width, hidden), BF), VM((width, hidden), BF), VM((2, hidden, H), BF),
-        VM((2, tokens, H), BF), VM((4, tokens, H), BF), VM((4, tokens, 128), F32),
+        VM((2, tokens, H), BF), VM((4, tokens, H), BF), VM((4, 8, tokens), F32),
         VM(((NEAR - 1) * TWO, H), BF), VM((NEAR * ONE, H), BF), VM((2, ep * TWO, H), BF),
         VM((ep * TWO, H), BF), VM((ep * TWO, H), BF), VM((ep * TWO, H), BF),
-        VM((NEAR * ONE, H), BF), VM((NEAR * ONE, H), BF),
-        VM(((NEAR - 1) * TWO, H), BF), VM((NEAR * ONE, H), BF),
-        VM((2 * tokens, H), F32), VM((2 * tokens, H), BF), VM((2 * tokens, H), BF), VM((2, tokens, H), BF),
-        VM((4 * tokens, NEAR * TWO), BF), VM((4 * tokens, NEAR * TWO), BF),
-        VM((2 * tokens, NEAR * ONE), BF), VM((2 * tokens, NEAR * ONE), BF),
+        VM((ep * ONE, H), BF), VM((ep * ONE, H), BF), VM((ep * ONE, H), BF), VM((2, tokens, H), BF),
+        VM((2 * tokens, ep * ONE), BF), VM((2 * tokens, ep * ONE), BF),
         VM((NEAR * TWO, 4 * tokens), BF),
         VM((z.blocks, size, BLOCK), BF), VM((z.blocks, size, dv), F32),
         VM((z.blocks, heads, BLOCK), F32), VM((z.blocks, BLOCK, 8), F32),
-        VM((z.stages, 2 * size, dv), BF), VM((z.stages, 2 * size, dv), BF), VM((size, dv), F32),
+        VM((z.stages, size + 16, dv), BF), VM((z.stages, size + 16, dv), BF), VM((size, dv), F32),
         VM((4, rows, depth), BF), VM((rows, features), BF),
         DMA((10,)), DMA((copies(z),)), DMA((copies(z),)), DMA((z.blocks + 1,)),
     ]
@@ -539,7 +556,7 @@
         cost_estimate=pl.CostEstimate(flops=10**10, bytes_accessed=20 << 20, transcendentals=0),
     )(
         query, keys, values, gate_pre, log_decay, out_weight.reshape(tp, depth, features), expert_input,
-        norm_gain.reshape(1, width), routes, route_weights, w_gate, w_up, w_down, spin, base,
+        norm_gain.reshape(1, width), routes.T, route_weights.T, w_gate, w_up, w_down, spin, base,
     )
 
 

time: 152 us -> 114 us (0.75)
  Pallas kernels: 145 us -> 109 us
  local copies, waits for them, and re-layouts: 6.7 us -> 3.93 us
    pallas_call x1, Pallas kernels: 145 us -> 109 us  [per_device(): pl.pallas_call(functools.partial(kernel, z), in_specs=[outside] * 4 + [in...]
    unnamed x6 -> x4, local copies, waits for them, and re-layouts: 6.7 us -> 3.93 us
where the time goes in v1:
time: 114 us
  Pallas kernels  109 us (96%)
  local copies, waits for them, and re-layouts  3.93 us (3%)
    pallas_call x1, Pallas kernels, per_device(): pl.pallas_call(functools.partial(kernel, z), in_specs=[outside] * 4 + [in...  109 us
    unnamed x4, local copies, waits for them, and re-layouts  3.93 us

profile of v1, /device:TPU:0, one launch (start us, length us, event | category | flops | bytes accessed | tf_op | source)
XLA Modules:
  0.0 114.0 jit_solution(12655357937587521231)
XLA Ops:
  0.6 109.4 %shard_map.158 = (bf16[1024,1024]{1,0:T(8,128)(2,1)}, bf16[64,4096]{1,0:T(8,128)(2,1)}) custom-call(bf16[1024,256]{1,0:T(8,128)(2,1)} %q_hbm.1, bf16[1024,256]{1,0:T(8,128)(2,1)} %k_hbm.1, bf16[1024,512]{1,0:T(8,128)(2,1)} %v_hbm.1, bf16[1024,512]{1,0:T(8,128)(2,1)} %g_hbm.1, f32[4,1024]{1,0:T(4,128)} %decay_ref.1, bf16[4,512,1024]{2,1,0:T(8,128)(2,1)} %bitcast.4, ...), custom_call_target="tpu_custom_call" | custom-call | flops 10000000000 | bytes 20971520 | tf_op jit(solution)/shard_map/pallas_call | solution.py:544
  110.1 0.0 copy-start
  110.1 3.1 %copy.19 = bf16[1024,1024]{1,0:T(8,128)(2,1)} copy(bf16[1024,1024]{1,0:T(8,128)(2,1)} %get-tuple-element.4) | data formatting | bytes 4194304
  113.2 0.0 copy-done
  113.2 0.8 copy.20
Async XLA Ops:
  110.1 3.1 %copy-start = (bf16[64,4096]{1,0:T(8,128)(2,1)S(1)}, bf16[64,4096]{1,0:T(8,128)(2,1)}, u32[]{:S(2)}) copy-start(bf16[64,4096]{1,0:T(8,128)(2,1)} %get-tuple-element.5) | copy-start | bytes 1572868

commit v2 on v1

--- a/solution.py
+++ b/solution.py
@@ -102,15 +102,19 @@
         load("wd%d" % h, wd_hbm.at[0, :, pl.ds(h * H, H)], wd_v.at[h])
     load("wo", wo_hbm, wo_v)
 
-    def send(src, dst, device):
+    def prepare(src, dst, device):
         i = used[0]
         used[0] += 1
         copy = pltpu.make_async_remote_copy(
             src_ref=src, dst_ref=dst, send_sem=send_sem.at[i], recv_sem=recv_sem.at[i],
             device_id=device, device_id_type=MESH,
         )
+        sent.append(copy)
+        return copy
+
+    def send(src, dst, device):
+        copy = prepare(src, dst, device)
         copy.start()
-        sent.append(copy)
         return copy
 
     both = jnp.concatenate([routes_ref[...].astype(F32), rweight_ref[...]], axis=0)
@@ -251,17 +255,25 @@
     for col in range(0, H, COLS):
         rows = jnp.concatenate([nb[g, :, col : col + COLS] for g in range(2)], axis=0)
         sc[:, col : col + COLS] = dot(placing, rows).astype(BF)
-    far_in = {}
+    far_in = [
+        prepare(sc.at[pl.ds(d * ONE, ONE)], xf.at[c, pl.ds((NEAR + d) * TWO, ONE)], (flip(e, NEAR + d), t))
+        for d in range(NEAR)
+    ]
 
     def far_send(d):
-        far_in[d] = send(
-            sc.at[pl.ds(d * ONE, ONE)], xf.at[c, pl.ds((NEAR + d) * TWO, ONE)], (flip(e, NEAR + d), t)
-        )
+        far_in[d].start()
 
     quarter = z.ep // 4
     first = list(range(quarter))
     second = list(range(quarter, NEAR))
     cut = max(1, quarter // 2)
+    outer = lax.rem(lax.div(e, NEAR), 2) == lax.rem(lax.div(e, max(1, NEAR // 2)), 2)
+
+    @pl.when(jnp.logical_not(outer))
+    def _():
+        for d in second[:cut]:
+            far_send(d)
+
     for s in range(1, z.stages):
         group, fade, prefix, prefade = scan_recv(s - 1, group, fade, prefix, prefade)
         scan_send(s)
@@ -291,7 +303,9 @@
         near_in[d].wait_recv()
         to_pair(d * TWO, TWO)
 
-    own_gate, near_gate, far_gate = [], [], []
+    near_gate, far_gate = [], []
+    pieces = [(b * BLOCK, BLOCK) for b in range(z.blocks - 1)]
+    pieces += [(z.rows - BLOCK + h * (BLOCK // 2), BLOCK // 2) for h in range(2)]
 
     @phase("mix")
     def mix(b, state):
@@ -324,16 +338,24 @@
 
     @phase("gate_x")
     def gate_x(b):
-        at = pl.ds(b * BLOCK, BLOCK)
-        far_gate.append(send(gate_all.at[0, at], gate_all.at[2, at], cross))
-        near_gate.append(send(gate_all.at[0, at], gate_all.at[1, at], pair))
+        gate_ready(b)
+        gate_start(b)
+
+    def gate_ready(b):
+        at = pl.ds(*pieces[b])
+        far_gate.append(prepare(gate_all.at[0, at], gate_all.at[2, at], cross))
+        near_gate.append(prepare(gate_all.at[0, at], gate_all.at[1, at], pair))
+
+    def gate_start(b):
+        far_gate[b].start()
+        near_gate[b].start()
 
     last_gate = []
 
     @phase("gate_on")
     def gate_on(b):
         far_gate[b].wait_recv()
-        at = pl.ds(b * BLOCK, BLOCK)
+        at = pl.ds(*pieces[b])
         last_gate.append(send(gate_all.at[2, at], gate_all.at[3, at], pair))
 
     stores = []
@@ -342,12 +364,11 @@
     def project(b):
         near_gate[b].wait_recv()
         last_gate[b].wait_recv()
-        at = slice(b * BLOCK, (b + 1) * BLOCK)
+        at = pl.ds(*pieces[b])
         sum_ = dot(gate_all[0, at], wo_v[t])
         for g in range(1, 4):
             sum_ = sum_ + dot(gate_all[g, at], wo_v[flip(t, g)])
         mix_v[at, :] = sum_.astype(BF)
-        at = pl.ds(b * BLOCK, BLOCK)
         copy = pltpu.make_async_copy(mix_v.at[at], mixed_hbm.at[at], out_sem.at[len(stores)])
         copy.start()
         stores.append(copy)
@@ -383,9 +404,12 @@
 
     cross_sum, home_out = {}, {}
 
-    @phase("back")
     def back(part):
         core_sum(part)
+        push(part)
+
+    @phase("back")
+    def push(part):
         for d in range(part * quarter, (part + 1) * quarter):
             cross_sum[d] = send(yk.at[pl.ds(d * TWO + ONE, ONE)], xr.at[pl.ds(d * ONE, ONE)], cross)
 
@@ -422,14 +446,23 @@
     for d in range(1, NEAR):
         near_in[d] = send(sn.at[pl.ds((d - 1) * TWO, TWO)], xf.at[c, pl.ds(d * TWO, TWO)], (flip(e, d), t))
         if d == NEAR - 2:
-            for i in second[:cut]:
+
+            @pl.when(outer)
+            def _():
+                for i in second[:cut]:
+                    far_send(i)
+
+            for i in second[cut:]:
                 far_send(i)
-    for i in second[cut:]:
-        far_send(i)
     to_pair(0, TWO)
 
     state = mix(1, state)
-    gate_x(1)
+    gate_ready(1)
+
+    @pl.when(outer)
+    def _():
+        gate_start(1)
+
     state = mix(2, state)
     for d in first[:cut]:
         relay(d)
@@ -439,6 +472,11 @@
             loads[name].wait()
     for d in first[cut:]:
         relay(d)
+
+    @pl.when(jnp.logical_not(outer))
+    def _():
+        gate_start(1)
+
     gate_x(2)
     for d in first:
         relay_on(d)
@@ -453,26 +491,28 @@
         relay(d)
     for d in range(quarter, NEAR):
         relay_near(d)
+    wait_pairs(1)
+    ffn(1)
     home(2)
-    back(0)
     for d in second:
         relay_on(d)
+    back(1)
     wait_pairs(3)
     ffn(3)
-    wait_pairs(1)
-    ffn(1)
+    core_sum(0)
     back(3)
-    back(1)
+    push(0)
     gate_x(3)
-    home(0)
+    gate_x(4)
     with phase("wait_wo"):
         loads["wo"].wait()
     for b in range(3):
         gate_on(b)
+    home(1)
     project(0)
     home(3)
     project(1)
-    home(1)
+    home(0)
     project(2)
 
     with phase("wait_home"):
@@ -488,8 +528,10 @@
     copy = pltpu.make_async_copy(fin.at[c], moe_hbm.at[:, mine], out_sem.at[len(stores)])
     copy.start()
     stores.append(copy)
-    gate_on(3)
-    project(3)
+    for b in (3, 4):
+        gate_on(b)
+    for b in (3, 4):
+        project(b)
     with phase("wait_done"):
         done.wait_recv()
     with phase("wait_stores"):
@@ -501,7 +543,7 @@
 
 
 def copies(z):
-    return 6 + z.near + (z.near - 1) + z.stages + z.near * 4 + 3 * z.blocks + 4 + 2 * z.ep
+    return 6 + z.near + (z.near - 1) + z.stages + z.near * 4 + 3 * (z.blocks + 1) + 4 + 2 * z.ep
 
 
 def per_device(
@@ -539,7 +581,7 @@
         VM((z.blocks, heads, BLOCK), F32), VM((z.blocks, BLOCK, 8), F32),
         VM((z.stages, size + 16, dv), BF), VM((z.stages, size + 16, dv), BF), VM((size, dv), F32),
         VM((4, rows, depth), BF), VM((rows, features), BF),
-        DMA((10,)), DMA((copies(z),)), DMA((copies(z),)), DMA((z.blocks + 1,)),
+        DMA((10,)), DMA((copies(z),)), DMA((copies(z),)), DMA((z.blocks + 2,)),
     ]
     return pl.pallas_call(
         functools.partial(kernel, z),

time: 114 us -> 112 us (0.982); the launches traced: 114 us -> 110 us
  Pallas kernels: 109 us -> 106 us
    pallas_call x1, Pallas kernels: 109 us -> 106 us  [per_device(): pl.pallas_call(functools.partial(kernel, z), in_specs=[outside] * 4 + [in...]
where the time goes in v2:
time: 112 us; the launch traced here: 110 us
  Pallas kernels  106 us (95%)
  local copies, waits for them, and re-layouts  3.93 us (4%)
    pallas_call x1, Pallas kernels, per_device(): pl.pallas_call(functools.partial(kernel, z), in_specs=[outside] * 4 + [in...  106 us
    unnamed x4, local copies, waits for them, and re-layouts  3.93 us

profile of v2, /device:TPU:0, one launch (start us, length us, event | category | flops | bytes accessed | tf_op | source)
XLA Modules:
  0.0 110.1 jit_solution(3289630593511433802)
XLA Ops:
  0.6 105.5 %shard_map.158 = (bf16[1024,1024]{1,0:T(8,128)(2,1)}, bf16[64,4096]{1,0:T(8,128)(2,1)}) custom-call(bf16[1024,256]{1,0:T(8,128)(2,1)} %q_hbm.1, bf16[1024,256]{1,0:T(8,128)(2,1)} %k_hbm.1, bf16[1024,512]{1,0:T(8,128)(2,1)} %v_hbm.1, bf16[1024,512]{1,0:T(8,128)(2,1)} %g_hbm.1, f32[4,1024]{1,0:T(4,128)} %decay_ref.1, bf16[4,512,1024]{2,1,0:T(8,128)(2,1)} %bitcast.4, ...), custom_call_target="tpu_custom_call" | custom-call | flops 10000000000 | bytes 20971520 | tf_op jit(solution)/shard_map/pallas_call | solution.py:586
  106.2 0.0 copy-start
  106.2 3.1 %copy.19 = bf16[1024,1024]{1,0:T(8,128)(2,1)} copy(bf16[1024,1024]{1,0:T(8,128)(2,1)} %get-tuple-element.4) | data formatting | bytes 4194304
  109.3 0.0 copy-done
  109.3 0.8 copy.20
Async XLA Ops:
  106.2 3.1 %copy-start = (bf16[64,4096]{1,0:T(8,128)(2,1)S(1)}, bf16[64,4096]{1,0:T(8,128)(2,1)}, u32[]{:S(2)}) copy-start(bf16[64,4096]{1,0:T(8,128)(2,1)} %get-tuple-element.5) | copy-start | bytes 1572868
